TPU v7x, 32 devices: a whole 2x2x4 slice. The times are simulated.
32 devices in a mesh: dp: 4 (over y, x), kv: 4 (over z), tp: 2 (over core).
Axes of the slice: x: 2, y: 2, z: 4, core: 2. Of those that a mesh axis runs over, the one named last changes fastest.
Arguments:
- tokens: bfloat16 [32, 2048], P('dp', 'kv'), may hold values from -6 to 6
- pre_gain: float32 [2048], P('kv'), may hold values from 0.1 to 1.9
- query_weight: bfloat16 [2048, 1024], P('kv', 'tp'), may hold values from -0.125 to 0.125
- key_weight: bfloat16 [2048, 1024], P('kv', 'tp'), may hold values from -0.125 to 0.125
- value_weight: bfloat16 [2048, 1024], P('kv', 'tp'), may hold values from -0.125 to 0.125
- outgate_weight: bfloat16 [2048, 1024], P('kv', 'tp'), may hold values from -0.125 to 0.125
- input_gate_weight: bfloat16 [2048, 4], replicated, may hold values from -0.125 to 0.125
- forget_gate_weight: bfloat16 [2048, 4], replicated, may hold values from -0.125 to 0.125
- cache_keys: bfloat16 [32, 64, 1024], P(('dp', 'kv'), None, 'tp'), may hold values from -6 to 6
- cache_values: bfloat16 [32, 64, 1024], P(('dp', 'kv'), None, 'tp'), may hold values from -6 to 6
- cache_input: float32 [32, 64, 4], P(('dp', 'kv'), None, 'tp'), may hold values from -6 to 250
- cache_forget: float32 [32, 64, 4], P(('dp', 'kv'), None, 'tp'), may hold values from -0.7 to 0
- lengths: int32 [32], P(('dp', 'kv')), may hold values from 1 to 64, 819 in all
- state_matrix: float32 [32, 4, 256, 256], P(('dp', 'kv'), 'tp'), may hold values from -6 to 6
- state_norm: float32 [32, 4, 256], P(('dp', 'kv'), 'tp'), may hold values from -6 to 6
- state_max: float32 [32, 4], P(('dp', 'kv'), 'tp'), may hold values from -4 to 253
- head_gain: float32 [1024], P('tp'), may hold values from 0.1 to 1.9
- out_weight: bfloat16 [1024, 2048], P('tp', 'kv'), may hold values from -0.375 to 0.375
- mixer_gain: float32 [2048], replicated, may hold values from 0.1 to 1.9
- gate_weight: bfloat16 [2048, 5632], P(None, ('kv', 'tp')), may hold values from -0.125 to 0.125
- up_weight: bfloat16 [2048, 5632], P(None, ('kv', 'tp')), may hold values from -0.125 to 0.125
- down_weight: bfloat16 [5632, 2048], P(('kv', 'tp')), may hold values from -0.21875 to 0.21875
Outputs:
- layer_out: bfloat16 [32, 2048], P('dp', ('kv', 'tp'))
Inputs may be any that keep to these rules, and one draw needn't show every extreme that they name: `lengths`: positions from a sequence's length on take no part.
All inputs are finite; a program needn't handle non-finite values. No bound on the sum of `lengths` on one device may be relied on, other than what follows from the above.
Results may differ from a plain program's by a relative error of at most 0.018.
Values may be sent and summed in bfloat16 or wider, within the bound.
No kernel may reach another device: no remote copies, remote signals or barrier semaphores. Data moves between devices by JAX's collectives and lax.ppermute only.
A program may use at most 64 MiB of HBM per device.

v0:
```python
import jax
import jax.numpy as jnp
from jax import lax
from jax.sharding import PartitionSpec as P

EPS = 1e-06


def per_device(
    tokens,
    pre_gain,
    query_weight,
    key_weight,
    value_weight,
    outgate_weight,
    input_gate_weight,
    forget_gate_weight,
    cache_keys,
    cache_values,
    cache_input,
    cache_forget,
    lengths,
    state_matrix,
    state_norm,
    state_max,
    head_gain,
    out_weight,
    mixer_gain,
    gate_weight,
    up_weight,
    down_weight,
):
    col_width = tokens.shape[1]
    own_seqs = cache_keys.shape[0]
    block_len = cache_keys.shape[1]
    head_count = state_max.shape[1]
    head_size = state_norm.shape[2]
    shard_index = lax.axis_index("kv")
    half_index = lax.axis_index("tp")
    kv_count = lax.axis_size("kv")
    model_width = col_width * kv_count
    token_values = tokens.astype(jnp.float32)
    squares = jnp.sum(token_values * token_values, axis=1)
    normed = (token_values * pre_gain[None, :]).astype(jnp.bfloat16)
    corner = (shard_index * col_width, half_index * head_count)
    gate_pair = jnp.concatenate(
        [
            lax.dynamic_slice(input_gate_weight, corner, (col_width, head_count)),
            lax.dynamic_slice(forget_gate_weight, corner, (col_width, head_count)),
        ],
        axis=1,
    )

    def product(weight):
        return jnp.dot(normed, weight, preferred_element_type=jnp.float32)

    query_term = product(query_weight)
    key_term = product(key_weight)
    value_term = product(value_weight)
    outgate_term = product(outgate_weight)
    gate_term = product(gate_pair)
    square_totals = lax.psum(squares, "kv")
    query_sum, key_sum, value_sum, outgate_sum, gate_sum = (
        lax.psum_scatter(query_term, "kv", scatter_dimension=0, tiled=True),
        lax.psum_scatter(key_term, "kv", scatter_dimension=0, tiled=True),
        lax.psum_scatter(value_term, "kv", scatter_dimension=0, tiled=True),
        lax.psum_scatter(outgate_term, "kv", scatter_dimension=0, tiled=True),
        lax.psum_scatter(gate_term, "kv", scatter_dimension=0, tiled=True),
    )
    own_squares = lax.dynamic_slice_in_dim(square_totals, shard_index * own_seqs, own_seqs, 0)
    scale_first = lax.rsqrt(own_squares / model_width + EPS)[:, None]
    query = (scale_first * query_sum).astype(jnp.bfloat16)
    keys_new = (scale_first * key_sum).astype(jnp.bfloat16)
    values_new = (scale_first * value_sum).astype(jnp.bfloat16)
    outgate = (scale_first * outgate_sum).astype(jnp.bfloat16)
    gate_values = scale_first * gate_sum
    in_gate = gate_values[:, :head_count]
    forget_new = jax.nn.log_sigmoid(gate_values[:, head_count:])
    query_heads = query.reshape(own_seqs, head_count, head_size)
    key_heads = keys_new.reshape(own_seqs, head_count, head_size)
    value_heads = values_new.reshape(own_seqs, head_count, head_size)
    cached_keys = cache_keys.reshape(own_seqs, block_len, head_count, head_size)
    cached_values = cache_values.reshape(own_seqs, block_len, head_count, head_size)
    inv_root = head_size ** (-0.5)
    live_mask = (lax.broadcasted_iota(jnp.int32, (own_seqs, block_len), 1) < lengths[:, None])[
        :, :, None
    ]
    forget_live = jnp.where(live_mask, cache_forget, jnp.float32(0.0))
    running = jnp.cumsum(forget_live, axis=1)
    total_log = running[:, -1, :] + forget_new
    weight_log = jnp.where(live_mask, total_log[:, None, :] - running + cache_input, -jnp.inf)
    state_log = total_log + state_max
    peak_log = jnp.maximum(jnp.maximum(state_log, in_gate), jnp.max(weight_log, axis=1))
    key_dots = (
        jnp.einsum("shd,slhd->slh", query_heads, cached_keys, preferred_element_type=jnp.float32)
        * inv_root
    )
    block_scores = jnp.exp(weight_log - peak_log[:, None, :]) * key_dots
    query_scaled = query_heads.astype(jnp.float32) * inv_root
    self_score = jnp.exp(in_gate - peak_log) * jnp.sum(
        query_scaled * key_heads.astype(jnp.float32), axis=2
    )
    carried = jnp.exp(state_log - peak_log)
    block_weights = block_scores.astype(jnp.bfloat16)
    memory_read = jnp.einsum(
        "shvd,shd->shv", state_matrix, query_scaled, precision=lax.Precision.HIGHEST
    )
    norm_read = jnp.einsum("shd,shd->sh", state_norm, query_scaled, precision=lax.Precision.HIGHEST)
    numerator = (
        carried[:, :, None] * memory_read
        + jnp.einsum(
            "slh,slhd->shd", block_weights, cached_values, preferred_element_type=jnp.float32
        )
        + self_score[:, :, None] * value_heads.astype(jnp.float32)
    )
    denominator = carried * norm_read + jnp.sum(block_scores, axis=1) + self_score
    hidden = numerator / jnp.maximum(jnp.abs(denominator), 1.0)[:, :, None]
    mixed_heads = (
        hidden.reshape(own_seqs, head_count * head_size)
        * head_gain[None, :]
        * jax.nn.sigmoid(outgate.astype(jnp.float32))
    ).astype(jnp.bfloat16)
    mix_terms = jnp.dot(
        lax.all_gather(mixed_heads, "kv", axis=0, tiled=True),
        out_weight,
        preferred_element_type=jnp.float32,
    )
    mix_sum = lax.psum_scatter(
        mix_terms.astype(jnp.bfloat16), "tp", scatter_dimension=1, tiled=True
    ).astype(jnp.float32)
    narrow = mix_sum.shape[1]
    residual = (
        lax.dynamic_slice_in_dim(token_values, half_index * narrow, narrow, 1) + mix_sum
    ).astype(jnp.bfloat16)
    piece_wide = lax.all_gather(residual, ("kv", "tp"), axis=1, tiled=True).astype(jnp.float32)
    normed_piece = (piece_wide * mixer_gain[None, :]).astype(jnp.bfloat16)
    gate_acc = jnp.dot(normed_piece, gate_weight, preferred_element_type=jnp.float32)
    up_acc = jnp.dot(normed_piece, up_weight, preferred_element_type=jnp.float32)
    sum_squares = jnp.sum(piece_wide * piece_wide, axis=1)
    gate_acc, up_acc, sum_squares = (gate_acc, up_acc, sum_squares)
    scale_mid = lax.rsqrt(sum_squares / model_width + EPS)[:, None]
    hidden_units = (jax.nn.silu(scale_mid * gate_acc) * (scale_mid * up_acc)).astype(jnp.bfloat16)
    summed = lax.psum_scatter(
        lax.dot_general(
            down_weight, hidden_units, (((0,), (1,)), ((), ())), preferred_element_type=jnp.float32
        ),
        ("kv", "tp"),
        scatter_dimension=0,
        tiled=True,
    )
    mixer_out = summed.T
    return (residual.astype(jnp.float32) + mixer_out).astype(jnp.bfloat16)


def solution(mesh):
    in_specs = (
        P("dp", "kv"),
        P("kv"),
        P("kv", "tp"),
        P("kv", "tp"),
        P("kv", "tp"),
        P("kv", "tp"),
        P(),
        P(),
        P(("dp", "kv"), None, "tp"),
        P(("dp", "kv"), None, "tp"),
        P(("dp", "kv"), None, "tp"),
        P(("dp", "kv"), None, "tp"),
        P(("dp", "kv")),
        P(("dp", "kv"), "tp", None, None),
        P(("dp", "kv"), "tp", None),
        P(("dp", "kv"), "tp"),
        P("tp"),
        P("tp", "kv"),
        P(),
        P(None, ("kv", "tp")),
        P(None, ("kv", "tp")),
        P(("kv", "tp"), None),
    )
    out_specs = P("dp", ("kv", "tp"))
    return jax.shard_map(
        per_device, mesh=mesh, in_specs=in_specs, out_specs=out_specs, check_vma=False
    )
```

profile of v0, /device:TPU:0, one launch (start us, length us, event | category | flops | bytes accessed | tf_op | source)
XLA Modules:
  0.0 147.6 jit_solution(3637259032463186697)
XLA Ops:
  6.5 0.0 copy-start
  6.5 0.0 all-reduce.8.cloned.1.call-start
  6.6 1.6 %multiply_reduce_fusion = f32[8]{0:T(128)} fusion(bf16[8,512]{1,0:T(8,128)(2,1)} %param.22), kind=kLoop, calls=%fused_computation.22 | loop fusion | flops 12280 | bytes 8224 | tf_op jit(solution)/shard_map/reduce_sum | solution.py:43
  8.2 1.9 %fusion.43 = f32[8,512]{1,0:T(8,128)} fusion(bf16[512,512]{1,0:T(8,128)(2,1)} %param.27, f32[512]{0:T(512)} %param.23, bf16[8,512]{1,0:T(8,128)(2,1)} %param.22), kind=kOutput, calls=%fused_computation.73 | convolution fusion | flops 4206592 | bytes 550912 | tf_op jit(solution)/shard_map/dot_general | solution.py:55
  10.0 1.9 %fusion.44 = f32[8,512]{1,0:T(8,128)} fusion(bf16[512,512]{1,0:T(8,128)(2,1)} %param.26, f32[512]{0:T(512)} %param.23, bf16[8,512]{1,0:T(8,128)(2,1)} %param.22), kind=kOutput, calls=%fused_computation.74 | convolution fusion | flops 4206592 | bytes 550912 | tf_op jit(solution)/shard_map/dot_general | solution.py:55
  11.9 1.9 %fusion.46 = f32[8,512]{1,0:T(8,128)} fusion(bf16[512,512]{1,0:T(8,128)(2,1)} %param.24, f32[512]{0:T(512)} %param.23, bf16[8,512]{1,0:T(8,128)(2,1)} %param.22), kind=kOutput, calls=%fused_computation.76 | convolution fusion | flops 4206592 | bytes 550912 | tf_op jit(solution)/shard_map/dot_general | solution.py:55
  13.7 0.8 dynamic_slice.15
  14.5 0.8 dynamic_slice.14
  15.3 1.9 %fusion.45 = f32[8,512]{1,0:T(8,128)} fusion(bf16[512,512]{1,0:T(8,128)(2,1)} %param.25, f32[512]{0:T(512)} %param.23, bf16[8,512]{1,0:T(8,128)(2,1)} %param.22), kind=kOutput, calls=%fused_computation.75 | convolution fusion | flops 4206592 | bytes 550912 | tf_op jit(solution)/shard_map/dot_general | solution.py:55
  17.1 1.4 fusion.21
  18.5 0.0 all-reduce.8.cloned.1.call-update
  18.6 0.0 reduce-scatter.3.cloned.1.call-start
  18.6 0.7 iota_compare_fusion
  19.3 0.7 broadcast_select_fusion
  20.0 0.0 copy-done.4
  20.0 0.1 copy.39
  20.1 0.1 reduce_window_sum.11
  20.2 0.1 copy.40
  20.3 1.3 dynamic-slice
  22.3 34.1 %all-reduce.8.cloned.1.call-done = (f32[8,512]{1,0:T(8,128)}, f32[8]{0:T(128)}, f32[8,512]{1,0:T(8,128)}, f32[8,512]{1,0:T(8,128)}, f32[8,4]{1,0:T(8,128)}, /*index=5*/f32[8,512]{1,0:T(8,128)}) async-done(((f32[8,512]{1,0:T(8,128)}, f32[8]{0:T(128)}, f32[8,512]{1,0:T(8,128)}, f32[8,512]{1,0:T(8,128)}, f32[8,4]{1,0:T(8,128)}, /*index=5*/f32[8,512]{1,0:T(8,128)}), (f32[8,512]{1,0:T(8,128)}, f32[8]{0:T(128)}, ...) | async-done | bytes 65712
  56.3 0.7 add_rsqrt_fusion.1
  57.1 0.8 fusion.37
  57.9 0.7 fusion.40
  58.7 1.0 fusion.5
  59.7 0.1 fusion.42
  59.8 0.9 fusion.49
  60.7 0.7 maximum_maximum_fusion
  61.4 0.8 fusion.50
  62.2 1.0 fusion.2
  63.2 0.8 multiply_reduce_fusion.1
  64.0 2.2 %fusion.31 = f32[2,2,1,256]{3,2,1,0:T(1,128)S(1)} fusion(f32[2,2,256,256]{3,2,1,0:T(8,128)} %param.35, f32[2,2,256,1]{2,1,0,3:T(2,128)S(1)} %get-tuple-element.20), kind=kOutput, calls=%fused_computation.46 | convolution fusion | flops 3145728 | bytes 1056768 | tf_op jit(solution)/shard_map/shvd,shd->shv/dot_general | solution.py:105
  66.2 0.1 fusion.35
  66.3 0.8 fusion.39
  67.1 12.0 %all-gather = bf16[4,2,512]{2,1,0:T(2,128)(2,1)S(1)} all-gather(bf16[1,2,512]{2,1,0:T(2,128)(2,1)S(1)} %fusion.39), channel_id=1, replica_groups=mesh['dp'=4,'kv'=4,'tp'=2] {'kv'}, dimensions={0}, use_global_device_ids=true | all-gather | bytes 10240 | tf_op jit(solution)/shard_map/all_gather | solution.py:124
  79.1 0.8 convolution_convert_fusion
  79.9 0.0 reduce-scatter.3.cloned.1.call-update
  79.9 0.0 reduce-scatter.5.cloned.1.call-start
  80.0 0.0 copy-done.2
  80.0 6.4 %reduce-scatter.3.cloned.1.call-done = bf16[8,256]{1,0:T(8,128)(2,1)} async-done(((bf16[8,512]{1,0:T(8,128)(2,1)}), bf16[8,256]{1,0:T(8,128)(2,1)}) %reduce-scatter.3.cloned.1.call-update) | async-done | bytes 4112 | tf_op jit(solution)/shard_map/reduce_scatter | solution.py:128
  86.3 0.7 add_convert_fusion
  87.0 14.3 %all_gather.7 = bf16[8,2048]{1,0:T(8,128)(2,1)S(1)} all-gather(bf16[8,256]{1,0:T(8,128)(2,1)S(1)} %add_convert_fusion), channel_id=1, replica_groups=mesh['dp'=4,'kv'=4,'tp'=2] {'kv','tp'}, dimensions={1}, use_global_device_ids=true | all-gather | bytes 36864 | tf_op jit(solution)/shard_map/all_gather | solution.py:135
  101.3 0.1 fusion.8
  101.5 2.7 %convolution_multiply_fusion.1 = f32[8,704]{1,0:T(8,128)S(1)} fusion(bf16[2048,704]{0,1:T(8,128)(2,1)} %param.41, bf16[8,2048]{1,0:T(8,128)(2,1)S(1)} %all_gather.7, f32[2048]{0:T(1024)S(1)} %copy-done.3, f32[8]{0:T(128)S(1)} %add_rsqrt_fusion), kind=kOutput, calls=%fused_computation.3 | convolution fusion | flops 23123456 | bytes 2947104 | tf_op jit(solution)/shard_map/dot_general | solution.py:137
  104.2 0.0 copy-done
  104.2 4.1 %convolution_bitcast_fusion = f32[2048,8]{0,1:T(8,128)} fusion(bf16[704,2048]{1,0:T(8,128)(2,1)S(1)} %copy-done, bf16[2048,704]{0,1:T(8,128)(2,1)} %param.42, bf16[8,2048]{1,0:T(8,128)(2,1)S(1)} %all_gather.7, f32[2048]{0:T(1024)S(1)} %copy-done.3, f32[8,704]{1,0:T(8,128)S(1)} %convolution_multiply_fusion.1, f32[8]{0:T(128)S(1)} %add_rsqrt_fusion), kind=kOutput, calls=%fused_computation | convolution fusion | flops 46225920 | bytes 5896224 | tf_op jit(solution)/shard_map/dot_general | solution.py:144
  108.3 0.0 reduce-scatter.5.cloned.1.call-update
  108.3 31.5 %reduce-scatter.5.cloned.1.call-done = f32[256,8]{0,1:T(8,128)} async-done(((f32[2048,8]{0,1:T(8,128)}), f32[256,8]{0,1:T(8,128)}) %reduce-scatter.5.cloned.1.call-update) | async-done | bytes 8208 | tf_op jit(solution)/shard_map/reduce_scatter | solution.py:143
  139.8 1.3 fusion.20
  (16 shorter events, 0.1 us)
Async XLA Ops:
  6.5 97.6 %copy-start = (bf16[704,2048]{1,0:T(8,128)(2,1)S(1)}, bf16[704,2048]{1,0:T(8,128)(2,1)}, u32[]{:S(2)}) copy-start(bf16[704,2048]{1,0:T(8,128)(2,1)} %param.43) | copy-start | bytes 8650756
  6.5 73.4 %copy-start.2 = (bf16[8,512]{1,0:T(8,128)(2,1)S(1)}, bf16[8,512]{1,0:T(8,128)(2,1)}, u32[]{:S(2)}) copy-start(bf16[8,512]{1,0:T(8,128)(2,1)} %param.22) | copy-start | bytes 24580
  6.5 72.6 %copy-start.1 = (bf16[512,512]{1,0:T(8,128)(2,1)S(1)}, bf16[512,512]{1,0:T(8,128)(2,1)}, u32[]{:S(2)}) copy-start(bf16[512,512]{1,0:T(8,128)(2,1)} %param.39) | copy-start | bytes 1572868
  6.5 94.9 %copy-start.3 = (f32[2048]{0:T(1024)S(1)}, f32[2048]{0:T(1024)}, u32[]{:S(2)}) copy-start(f32[2048]{0:T(1024)} %param.40) | copy-start | bytes 24580
  6.5 49.8 %all-reduce.8.cloned.1.call-start = ((), (), s32[]{:S(2)}) async-start(), calls=%async_computation.4 | async-start | bytes 140288
  18.6 67.8 %reduce-scatter.3.cloned.1.call-start = ((), (), s32[]{:S(2)}) async-start(), calls=%async_computation.2 | async-start | bytes 12288 | tf_op jit(solution)/shard_map/reduce_scatter | solution.py:128
  19.3 0.7 copy-start.4
  79.9 59.9 %reduce-scatter.5.cloned.1.call-start = ((), (), s32[]{:S(2)}) async-start(), calls=%async_computation.3 | async-start | bytes 73728 | tf_op jit(solution)/shard_map/reduce_scatter | solution.py:143
Sparse Core Ops, SparseCore 0:
  18.7 37.6 all-reduce.7
  80.0 6.2 reduce-scatter.2
  108.4 31.2 reduce-scatter.4
where the time goes:
time: 149 us; the launch traced here: 148 us
  waiting for transfers between devices  71.9 us (48%)
  blocking collectives  26.3 us (18%)
  matrix products  20.6 us (14%)
  between operations  13.8 us (9%)
  other arithmetic  11.7 us (8%)
  local copies, waits for them, and re-layouts  3.11 us (2%)
    unnamed x4, waiting for transfers between devices  34.1 us
    reduce_scatter x1, waiting for transfers between devices, per_device(): lax.psum_scatter(lax.dot_general(down_weight, hidden_units, (((0,), (1,))...  31.5 us
    all_gather x1, blocking collectives, per_device(): lax.all_gather(residual, ('kv', 'tp'), axis=1, tiled=True)  14.3 us
    all_gather x1, blocking collectives, per_device(): lax.all_gather(mixed_heads, 'kv', axis=0, tiled=True)  12 us
    dot_general x5, matrix products, product(): return jnp.dot(normed, weight, preferred_element_type=jnp.float32)  8.84 us
    reduce_scatter x1, waiting for transfers between devices, per_device(): lax.psum_scatter(mix_terms.astype(jnp.bfloat16), 'tp', scatter_dimension=...  6.35 us
    dot_general x1, matrix products, per_device(): lax.dot_general(down_weight, hidden_units, (((0,), (1,)), ((), ())), pref...  4.12 us
  transfers between devices with their start and end apart: 3, of which 3 were waited for; matrix products, arithmetic and copies ran while one was open for 2% of the time, Pallas kernels for 0%

commit v1 on v0

--- a/solution.py
+++ b/solution.py
@@ -4,6 +4,18 @@
 from jax.sharding import PartitionSpec as P
 
 EPS = 1e-06
+
+
+def gather_by_bits(array, axis, dim):
+    ways, here = (lax.axis_size(axis), lax.axis_index(axis))
+    grown, reach = (array, 1)
+    while reach < ways:
+        theirs = lax.ppermute(grown, axis, [(d, d ^ reach) for d in range(ways)])
+        mine_first = jnp.concatenate([grown, theirs], axis=dim)
+        theirs_first = jnp.concatenate([theirs, grown], axis=dim)
+        grown = jnp.where(here & reach == 0, mine_first, theirs_first)
+        reach = 2 * reach
+    return grown
 
 
 def per_device(
@@ -121,9 +133,7 @@
         * jax.nn.sigmoid(outgate.astype(jnp.float32))
     ).astype(jnp.bfloat16)
     mix_terms = jnp.dot(
-        lax.all_gather(mixed_heads, "kv", axis=0, tiled=True),
-        out_weight,
-        preferred_element_type=jnp.float32,
+        gather_by_bits(mixed_heads, "kv", 0), out_weight, preferred_element_type=jnp.float32
     )
     mix_sum = lax.psum_scatter(
         mix_terms.astype(jnp.bfloat16), "tp", scatter_dimension=1, tiled=True

time: 149 us -> 146 us (0.980)
  blocking collectives: 26.3 us -> 14.3 us
  waiting for transfers between devices: 71.9 us -> 77.5 us
  starting transfers between devices: 0.12 us -> 4.21 us
    all_gather x1 -> x0, blocking collectives: 12 us -> none  [per_device(): lax.all_gather(mixed_heads, 'kv', axis=0, tiled=True)]
    ppermute x0 -> x2, waiting for transfers between devices: none -> 4.12 us  [gather_by_bits(): theirs = lax.ppermute(grown, axis, [(d, d ^ reach) for d in range(ways)])]
    ppermute x0 -> x2, starting transfers between devices: none -> 4.1 us  [gather_by_bits(): theirs = lax.ppermute(grown, axis, [(d, d ^ reach) for d in range(ways)])]
  transfers between devices with their start and end apart: 3 -> 5, of which waited for: 3 -> 5; matrix products, arithmetic and copies ran while one was open for 2% -> 2% of each run, Pallas kernels for 0% -> 0%
where the time goes in v1:
time: 146 us; the launch traced here: 145 us
  waiting for transfers between devices  77.5 us (53%)
  matrix products  20.6 us (14%)
  blocking collectives  14.3 us (10%)
  between operations  13.8 us (9%)
  other arithmetic  11.7 us (8%)
  starting transfers between devices  4.21 us (3%)
  local copies, waits for them, and re-layouts  3.1 us (2%)
    unnamed x4, waiting for transfers between devices  34.1 us
    reduce_scatter x1, waiting for transfers between devices, per_device(): lax.psum_scatter(lax.dot_general(down_weight, hidden_units, (((0,), (1,))...  31.5 us
    all_gather x1, blocking collectives, per_device(): lax.all_gather(residual, ('kv', 'tp'), axis=1, tiled=True)  14.3 us
    dot_general x5, matrix products, product(): return jnp.dot(normed, weight, preferred_element_type=jnp.float32)  8.84 us
    reduce_scatter x1, waiting for transfers between devices, per_device(): lax.psum_scatter(mix_terms.astype(jnp.bfloat16), 'tp', scatter_dimension=...  7.67 us
    ppermute x2, waiting for transfers between devices, gather_by_bits(): theirs = lax.ppermute(grown, axis, [(d, d ^ reach) for d in range(ways)])  4.12 us
    dot_general x1, matrix products, per_device(): lax.dot_general(down_weight, hidden_units, (((0,), (1,)), ((), ())), pref...  4.12 us
    ppermute x2, starting transfers between devices, gather_by_bits(): theirs = lax.ppermute(grown, axis, [(d, d ^ reach) for d in range(ways)])  4.1 us
  transfers between devices with their start and end apart: 5, of which 5 were waited for; matrix products, arithmetic and copies ran while one was open for 2% of the time, Pallas kernels for 0%

profile of v1, /device:TPU:0, one launch (start us, length us, event | category | flops | bytes accessed | tf_op | source)
XLA Modules:
  0.0 145.3 jit_solution(15174428867666934797)
XLA Ops:
  6.5 0.0 all-reduce.8.cloned.1.call-start
  6.6 1.6 %multiply_reduce_fusion = f32[8]{0:T(128)} fusion(bf16[8,512]{1,0:T(8,128)(2,1)} %param.22), kind=kLoop, calls=%fused_computation.22 | loop fusion | flops 12280 | bytes 8224 | tf_op jit(solution)/shard_map/reduce_sum | solution.py:55
  8.2 1.9 %fusion.49 = f32[8,512]{1,0:T(8,128)} fusion(bf16[512,512]{1,0:T(8,128)(2,1)} %param.26, f32[512]{0:T(512)} %param.23, bf16[8,512]{1,0:T(8,128)(2,1)} %param.22), kind=kOutput, calls=%fused_computation.81 | convolution fusion | flops 4206592 | bytes 550912 | tf_op jit(solution)/shard_map/dot_general | solution.py:67
  10.0 1.9 %fusion.51 = f32[8,512]{1,0:T(8,128)} fusion(bf16[512,512]{1,0:T(8,128)(2,1)} %param.24, f32[512]{0:T(512)} %param.23, bf16[8,512]{1,0:T(8,128)(2,1)} %param.22), kind=kOutput, calls=%fused_computation.83 | convolution fusion | flops 4206592 | bytes 550912 | tf_op jit(solution)/shard_map/dot_general | solution.py:67
  11.9 0.8 dynamic_slice.15
  12.6 0.8 dynamic_slice.14
  13.4 1.9 %fusion.50 = f32[8,512]{1,0:T(8,128)} fusion(bf16[512,512]{1,0:T(8,128)(2,1)} %param.25, f32[512]{0:T(512)} %param.23, bf16[8,512]{1,0:T(8,128)(2,1)} %param.22), kind=kOutput, calls=%fused_computation.82 | convolution fusion | flops 4206592 | bytes 550912 | tf_op jit(solution)/shard_map/dot_general | solution.py:67
  15.3 1.9 %fusion.48 = f32[8,512]{1,0:T(8,128)} fusion(bf16[512,512]{1,0:T(8,128)(2,1)} %param.27, f32[512]{0:T(512)} %param.23, bf16[8,512]{1,0:T(8,128)(2,1)} %param.22), kind=kOutput, calls=%fused_computation.80 | convolution fusion | flops 4206592 | bytes 550912 | tf_op jit(solution)/shard_map/dot_general | solution.py:67
  17.1 1.4 fusion.27
  18.5 0.0 all-reduce.8.cloned.1.call-update
  18.6 0.0 reduce-scatter.3.cloned.1.call-start
  18.6 0.7 iota_compare_fusion
  19.3 0.7 broadcast_select_fusion
  20.0 0.1 copy.39
  20.1 0.1 reduce_window_sum.11
  20.2 0.1 copy.40
  20.3 1.3 dynamic-slice
  22.3 34.1 %all-reduce.8.cloned.1.call-done = (f32[8,512]{1,0:T(8,128)}, f32[8]{0:T(128)}, f32[8,512]{1,0:T(8,128)}, f32[8,4]{1,0:T(8,128)}, f32[8,512]{1,0:T(8,128)}, /*index=5*/f32[8,512]{1,0:T(8,128)}) async-done(((f32[8,512]{1,0:T(8,128)}, f32[8]{0:T(128)}, f32[8,512]{1,0:T(8,128)}, f32[8,4]{1,0:T(8,128)}, f32[8,512]{1,0:T(8,128)}, /*index=5*/f32[8,512]{1,0:T(8,128)}), (f32[8,512]{1,0:T(8,128)}, f32[8]{0:T(128)}, ...) | async-done | bytes 65712
  56.3 0.7 add_rsqrt_fusion.1
  57.1 0.8 fusion.43
  57.9 0.7 fusion.45
  58.7 1.0 fusion.5
  59.7 0.1 fusion.47
  59.8 0.9 fusion.55
  60.7 0.7 maximum_maximum_fusion
  61.4 0.8 fusion.56
  62.2 1.0 fusion.2
  63.3 0.8 multiply_reduce_fusion.1
  64.0 2.2 %fusion.37 = f32[2,2,1,256]{3,2,1,0:T(1,128)S(1)} fusion(f32[2,2,256,256]{3,2,1,0:T(8,128)} %param.35, f32[2,2,256,1]{2,1,0,3:T(2,128)S(1)} %get-tuple-element.20), kind=kOutput, calls=%fused_computation.54 | convolution fusion | flops 3145728 | bytes 1056768 | tf_op jit(solution)/shard_map/shvd,shd->shv/dot_general | solution.py:117
  66.2 0.1 fusion.41
  66.3 0.8 fusion.40
  67.1 1.6 %collective-permute-start = (bf16[2,512]{1,0:T(2,128)(2,1)S(1)}, bf16[2,512]{1,0:T(2,128)(2,1)S(1)}, u32[]{:S(2)}, u32[]{:S(2)}) collective-permute-start(bf16[2,512]{1,0:T(2,128)(2,1)S(1)} %fusion.40), channel_id=1, source_target_pairs={{0,2},{2,0},{4,6},{6,4},{1,3},{3,1},{5,7},{7,5},{8,10},{10,8},{12,... | collective-permute-start | bytes 6152 | tf_op jit(solution)/shard_map/ppermute | solution.py:13
  68.8 2.0 %collective-permute-done = bf16[2,512]{1,0:T(2,128)(2,1)S(1)} collective-permute-done((bf16[2,512]{1,0:T(2,128)(2,1)S(1)}, bf16[2,512]{1,0:T(2,128)(2,1)S(1)}, u32[]{:S(2)}, u32[]{:S(2)}) %collective-permute-start) | collective-permute-done | bytes 2080 | tf_op jit(solution)/shard_map/ppermute | solution.py:13
  70.8 2.5 %collective-permute-start.1 = (bf16[4,512]{1,0:T(4,128)(2,1)S(1)}, bf16[4,512]{1,0:T(4,128)(2,1)S(1)}, u32[]{:S(2)}, u32[]{:S(2)}) collective-permute-start(bf16[4,512]{1,0:T(4,128)(2,1)S(1)} %maximum_select_fusion.2), channel_id=1, source_target_pairs={{0,4},{2,6},{4,0},{6,2},{1,5},{3,7},{5,1},{7,3},{8,12},{10,14},{12... | collective-permute-start | bytes 12296 | tf_op jit(solution)/shard_map/ppermute | solution.py:13
  73.3 2.1 %collective-permute-done.1 = bf16[4,512]{1,0:T(4,128)(2,1)S(1)} collective-permute-done((bf16[4,512]{1,0:T(4,128)(2,1)S(1)}, bf16[4,512]{1,0:T(4,128)(2,1)S(1)}, u32[]{:S(2)}, u32[]{:S(2)}) %collective-permute-start.1) | collective-permute-done | bytes 4128 | tf_op jit(solution)/shard_map/ppermute | solution.py:13
  75.4 0.8 convolution_convert_fusion
  76.2 0.0 reduce-scatter.3.cloned.1.call-update
  76.2 0.0 reduce-scatter.5.cloned.1.call-start
  76.2 0.0 copy-done.2
  76.3 7.7 %reduce-scatter.3.cloned.1.call-done = bf16[8,256]{1,0:T(8,128)(2,1)} async-done(((bf16[8,512]{1,0:T(8,128)(2,1)}), bf16[8,256]{1,0:T(8,128)(2,1)}) %reduce-scatter.3.cloned.1.call-update) | async-done | bytes 4112 | tf_op jit(solution)/shard_map/reduce_scatter | solution.py:138
  83.9 0.7 add_convert_fusion
  84.6 14.3 %all_gather.3 = bf16[8,2048]{1,0:T(8,128)(2,1)S(1)} all-gather(bf16[8,256]{1,0:T(8,128)(2,1)S(1)} %add_convert_fusion), channel_id=1, replica_groups=mesh['dp'=4,'kv'=4,'tp'=2] {'kv','tp'}, dimensions={1}, use_global_device_ids=true | all-gather | bytes 36864 | tf_op jit(solution)/shard_map/all_gather | solution.py:145
  99.0 0.1 fusion.8
  99.1 2.7 %convolution_multiply_fusion.1 = f32[8,704]{1,0:T(8,128)S(1)} fusion(bf16[2048,704]{0,1:T(8,128)(2,1)} %param.41, bf16[8,2048]{1,0:T(8,128)(2,1)S(1)} %all_gather.3, f32[2048]{0:T(1024)S(1)} %copy-done.3, f32[8]{0:T(128)S(1)} %add_rsqrt_fusion), kind=kOutput, calls=%fused_computation.3 | convolution fusion | flops 23123456 | bytes 2947104 | tf_op jit(solution)/shard_map/dot_general | solution.py:147
  101.8 4.1 %convolution_bitcast_fusion = f32[2048,8]{0,1:T(8,128)} fusion(bf16[704,2048]{1,0:T(8,128)(2,1)S(1)} %copy-done, bf16[2048,704]{0,1:T(8,128)(2,1)} %param.42, bf16[8,2048]{1,0:T(8,128)(2,1)S(1)} %all_gather.3, f32[2048]{0:T(1024)S(1)} %copy-done.3, f32[8,704]{1,0:T(8,128)S(1)} %convolution_multiply_fusion.1, f32[8]{0:T(128)S(1)} %add_rsqrt_fusion), kind=kOutput, calls=%fused_computation | convolution fusion | flops 46225920 | bytes 5896224 | tf_op jit(solution)/shard_map/dot_general | solution.py:154
  105.9 0.0 reduce-scatter.5.cloned.1.call-update
  105.9 31.5 %reduce-scatter.5.cloned.1.call-done = f32[256,8]{0,1:T(8,128)} async-done(((f32[2048,8]{0,1:T(8,128)}), f32[256,8]{0,1:T(8,128)}) %reduce-scatter.5.cloned.1.call-update) | async-done | bytes 8208 | tf_op jit(solution)/shard_map/reduce_scatter | solution.py:153
  137.4 1.3 fusion.25
  (19 shorter events, 0.1 us)
Async XLA Ops:
  6.5 95.2 %copy-start = (bf16[704,2048]{1,0:T(8,128)(2,1)S(1)}, bf16[704,2048]{1,0:T(8,128)(2,1)}, u32[]{:S(2)}) copy-start(bf16[704,2048]{1,0:T(8,128)(2,1)} %param.43) | copy-start | bytes 8650756
  6.5 69.7 %copy-start.2 = (bf16[8,512]{1,0:T(8,128)(2,1)S(1)}, bf16[8,512]{1,0:T(8,128)(2,1)}, u32[]{:S(2)}) copy-start(bf16[8,512]{1,0:T(8,128)(2,1)} %param.22) | copy-start | bytes 24580
  6.5 68.8 %copy-start.1 = (bf16[512,512]{1,0:T(8,128)(2,1)S(1)}, bf16[512,512]{1,0:T(8,128)(2,1)}, u32[]{:S(2)}) copy-start(bf16[512,512]{1,0:T(8,128)(2,1)} %param.39) | copy-start | bytes 1572868
  6.5 92.6 %copy-start.3 = (f32[2048]{0:T(1024)S(1)}, f32[2048]{0:T(1024)}, u32[]{:S(2)}) copy-start(f32[2048]{0:T(1024)} %param.40) | copy-start | bytes 24580
  6.5 49.8 %all-reduce.8.cloned.1.call-start = ((), (), s32[]{:S(2)}) async-start(), calls=%async_computation.4 | async-start | bytes 140288
  18.6 65.4 %reduce-scatter.3.cloned.1.call-start = ((), (), s32[]{:S(2)}) async-start(), calls=%async_computation.2 | async-start | bytes 12288 | tf_op jit(solution)/shard_map/reduce_scatter | solution.py:138
  19.3 0.7 copy-start.4
  67.1 3.7 %collective-permute-start = (bf16[2,512]{1,0:T(2,128)(2,1)S(1)}, bf16[2,512]{1,0:T(2,128)(2,1)S(1)}, u32[]{:S(2)}, u32[]{:S(2)}) collective-permute-start(bf16[2,512]{1,0:T(2,128)(2,1)S(1)} %fusion.40), channel_id=1, source_target_pairs={{0,2},{2,0},{4,6},{6,4},{1,3},{3,1},{5,7},{7,5},{8,10},{10,8},{12,... | collective-permute-start | bytes 6152 | tf_op jit(solution)/shard_map/ppermute | solution.py:13
  70.8 4.6 %collective-permute-start.1 = (bf16[4,512]{1,0:T(4,128)(2,1)S(1)}, bf16[4,512]{1,0:T(4,128)(2,1)S(1)}, u32[]{:S(2)}, u32[]{:S(2)}) collective-permute-start(bf16[4,512]{1,0:T(4,128)(2,1)S(1)} %maximum_select_fusion.2), channel_id=1, source_target_pairs={{0,4},{2,6},{4,0},{6,2},{1,5},{3,7},{5,1},{7,3},{8,12},{10,14},{12... | collective-permute-start | bytes 12296 | tf_op jit(solution)/shard_map/ppermute | solution.py:13
  76.2 61.3 %reduce-scatter.5.cloned.1.call-start = ((), (), s32[]{:S(2)}) async-start(), calls=%async_computation.3 | async-start | bytes 73728 | tf_op jit(solution)/shard_map/reduce_scatter | solution.py:153
Sparse Core Ops, SparseCore 0:
  18.7 37.6 all-reduce.7
  76.3 7.5 reduce-scatter.2
  106.0 31.3 reduce-scatter.4
